TPU v7x, 32 devices: a whole 2x2x4 slice. The times are simulated.
32 devices in a mesh: sp: 4 (over y, x), tp: 8 (over z, core).
Axes of the slice: x: 2, y: 2, z: 4, core: 2. Of those that a mesh axis runs over, the one named last changes fastest.
Arguments:
- tokens: bfloat16 [2048, 4096], P('sp', 'tp'), may hold values from -6 to 6
- pre_gain: float32 [2, 4096], replicated, may hold values from 0.1 to 1.9
- w_value: bfloat16 [2, 4096, 4096], P(None, 'sp', 'tp'), may hold values from -0.09375 to 0.09375
- w_gate: bfloat16 [2, 4096, 4096], P(None, 'sp', 'tp'), may hold values from -0.09375 to 0.09375
- conv_taps: float32 [2, 31, 4096], P(None, None, 'tp'), may hold values from -3.5 to 3.5
- conv_bias: float32 [2, 4096], P(None, 'tp'), may hold values from -3 to 3
- norm_gain: float32 [2, 4096], P(None, 'tp'), may hold values from 0.1 to 1.9
- norm_bias: float32 [2, 4096], P(None, 'tp'), may hold values from -3 to 3
- w_out: bfloat16 [2, 4096, 4096], P(None, 'sp', 'tp'), may hold values from -0.09375 to 0.09375
- post_gain: float32 [2, 4096], P(None, 'tp'), may hold values from 0.1 to 1.9
Outputs:
- stream: bfloat16 [2048, 4096], P('sp', 'tp')
All inputs are finite; a program needn't handle non-finite values.
Results may differ from a plain program's by a relative error of at most 0.009.
Values may be sent and summed in bfloat16 or wider, within the bound.
A program may use at most 64 MiB of HBM per device.

v0:
```python
import jax
import jax.numpy as jnp
from jax import lax
from jax.sharding import PartitionSpec as P


def passed_along(value, axis, steps):
    count = lax.axis_size(axis)
    leading, last = (max(0, -steps), min(count, count - steps))
    return lax.ppermute(value, axis, [(source, source + steps) for source in range(leading, last)])


def shards(
    tokens, pre_gain, w_value, w_gate, conv_taps, conv_bias, norm_gain, norm_bias, w_out, post_gain
):
    layer_count = w_value.shape[0]
    tap_count = conv_taps.shape[1]
    channel_count = conv_taps.shape[2] * lax.axis_size("tp")
    model_width = tokens.shape[1] * lax.axis_size("tp")
    local_rows = tokens.shape[0]
    every_value, every_gate, every_out = (
        lax.all_gather(w_value, "sp", axis=1, tiled=True),
        lax.all_gather(w_gate, "sp", axis=1, tiled=True),
        lax.all_gather(w_out, "sp", axis=1, tiled=True),
    )
    stream = tokens
    for layer_index in range(layer_count):
        gathered = lax.all_gather(stream, "tp", axis=1, tiled=True)
        full_rows = gathered.astype(jnp.float32)
        scale_rows = lax.rsqrt(jnp.mean(full_rows * full_rows, axis=-1, keepdims=True) + 1e-06)
        normed = (full_rows * scale_rows * pre_gain[layer_index]).astype(jnp.bfloat16)
        value_block = every_value[layer_index]
        gate_block = every_gate[layer_index]
        out_block = every_out[layer_index]
        value_proj = jnp.dot(normed, value_block, preferred_element_type=jnp.float32)
        gate_proj = jnp.dot(normed, gate_block, preferred_element_type=jnp.float32)
        glu_out = (value_proj * jax.nn.sigmoid(gate_proj)).astype(jnp.bfloat16)
        earlier = passed_along(glu_out[local_rows - (tap_count - 1) :], "sp", 1)
        padded = jnp.concatenate([earlier, glu_out], axis=0).astype(jnp.float32)
        filtered = jnp.zeros(glu_out.shape, jnp.float32) + conv_bias[layer_index]
        for tap_index in range(tap_count):
            filtered = (
                filtered
                + padded[tap_index : tap_index + local_rows] * conv_taps[layer_index, tap_index]
            )
        channel_sum, channel_square = lax.psum(
            (jnp.sum(filtered, axis=-1), jnp.sum(filtered * filtered, axis=-1)), "tp"
        )
        centre = channel_sum / channel_count
        spread = jnp.maximum(channel_square / channel_count - centre * centre, 0.0)
        shaped = (filtered - centre[:, None]) * lax.rsqrt(spread + 1e-05)[:, None]
        mixed = jax.nn.silu(shaped * norm_gain[layer_index] + norm_bias[layer_index]).astype(
            jnp.bfloat16
        )
        whole_mixed = lax.all_gather(mixed, "tp", axis=1, tiled=True)
        branch_low = jnp.dot(whole_mixed, out_block, preferred_element_type=jnp.float32).astype(
            jnp.bfloat16
        )
        branch = lax.optimization_barrier(branch_low).astype(jnp.float32)
        total = lax.psum(jnp.sum(branch * branch, axis=-1), "tp")
        rescale = lax.rsqrt(total / model_width + 1e-06)[:, None]
        stream = (stream.astype(jnp.float32) + branch * rescale * post_gain[layer_index]).astype(
            jnp.bfloat16
        )
    return stream


def solution(mesh):
    in_specs = (
        P("sp", "tp"),
        P(),
        P(None, "sp", "tp"),
        P(None, "sp", "tp"),
        P(None, None, "tp"),
        P(None, "tp"),
        P(None, "tp"),
        P(None, "tp"),
        P(None, "sp", "tp"),
        P(None, "tp"),
    )
    out_specs = P("sp", "tp")
    return jax.shard_map(shards, mesh=mesh, in_specs=in_specs, out_specs=out_specs, check_vma=False)
```

profile of v0, /device:TPU:0, one launch (start us, length us, event | category | flops | bytes accessed | tf_op | source)
XLA Modules:
  0.0 551.2 jit_solution(2232420375245703278)
XLA Ops:
  9.6 49.0 %all-gather.8.cloned.1.call-done = bf16[512,4096]{1,0:T(8,128)(2,1)} async-done(((bf16[512,512]{1,0:T(8,128)(2,1)}), bf16[512,4096]{1,0:T(8,128)(2,1)}) %all-gather.8.cloned.1.call-update) | async-done | bytes 4194320 | tf_op jit(solution)/shard_map/all_gather | solution.py:28
  58.6 3.1 fusion
  61.7 85.1 %all-gather.12.cloned.1.call-done = bf16[2,4096,512]{2,1,0:T(8,128)(2,1)} async-done(((bf16[2,1024,512]{2,1,0:T(8,128)(2,1)}), bf16[2,4096,512]{2,1,0:T(8,128)(2,1)}) %all-gather.12.cloned.1.call-update) | async-done | bytes 8388624 | tf_op jit(solution)/shard_map/all_gather | solution.py:23
  146.7 6.0 %fusion.21 = f32[512,512]{1,0:T(8,128)S(1)} fusion(bf16[2,4096,512]{2,1,0:T(8,128)(2,1)} %all-gather.12.cloned.1.call-done, bf16[512,4096]{1,0:T(8,128)(2,1)} %all-gather.8.cloned.1.call-done, f32[4096]{0:T(1024)S(1)} %bitcast.122, f32[512]{0:T(512)S(1)} %add_rsqrt_fusion.5), kind=kOutput, calls=%fused_computation.35 | convolution fusion | flops 2156658688 | bytes 9455616 | tf_op jit(solution)/shard_map/dot_general | solution.py:36
  152.7 83.4 %all-gather.10.cloned.1.call-done = bf16[2,4096,512]{2,1,0:T(8,128)(2,1)} async-done(((bf16[2,1024,512]{2,1,0:T(8,128)(2,1)}), bf16[2,4096,512]{2,1,0:T(8,128)(2,1)}) %all-gather.10.cloned.1.call-update) | async-done | bytes 8388624 | tf_op jit(solution)/shard_map/all_gather | solution.py:22
  236.1 5.8 %fusion.23 = bf16[512,512]{1,0:T(8,128)(2,1)S(1)} fusion(f32[512,512]{1,0:T(8,128)S(1)} %fusion.21, bf16[2,4096,512]{2,1,0:T(8,128)(2,1)} %all-gather.10.cloned.1.call-done, bf16[512,4096]{1,0:T(8,128)(2,1)} %all-gather.8.cloned.1.call-done, f32[4096]{0:T(1024)S(1)} %bitcast.123, f32[512]{0:T(512)S(1)} %add_rsqrt_fusion.5), kind=kOutput, calls=%fused_computation.37 | convolution fusion | flops 2156396544 | bytes 9979904 | tf_op jit(solution)/shard_map/dot_general | solution.py:35
  242.0 3.4 collective-permute-start
  245.4 1.6 collective-permute-done
  247.1 5.0 fusion.101
  252.1 15.3 %all-reduce.1 = (f32[512]{0:T(512)S(1)}, f32[512]{0:T(512)S(1)}) all-reduce(f32[512]{0:T(512)S(1)} %get-tuple-element.8, f32[512]{0:T(512)S(1)} %get-tuple-element.7), channel_id=1, replica_groups=mesh['sp'=4,'tp'=8] {'tp'}, use_global_device_ids=true, to_apply=%region_4.0 | all-reduce | flops 1024 | bytes 8192 | tf_op jit(solution)/shard_map/psum | solution.py:46
  268.8 56.5 %all-gather.16.cloned.1.call-done = bf16[2,4096,512]{2,1,0:T(8,128)(2,1)} async-done(((bf16[2,1024,512]{2,1,0:T(8,128)(2,1)}), bf16[2,4096,512]{2,1,0:T(8,128)(2,1)}) %all-gather.16.cloned.1.call-update) | async-done | bytes 8388624 | tf_op jit(solution)/shard_map/all_gather | solution.py:24
  325.3 48.4 %all-gather.14.cloned.1.call-done = bf16[512,4096]{1,0:T(8,128)(2,1)} async-done(((bf16[512,512]{1,0:T(8,128)(2,1)}), bf16[512,4096]{1,0:T(8,128)(2,1)}) %all-gather.14.cloned.1.call-update) | async-done | bytes 4194320 | tf_op jit(solution)/shard_map/all_gather | solution.py:55
  373.7 5.8 %fusion.24 = bf16[512,512]{1,0:T(8,128)(2,1)S(1)} fusion(bf16[512,4096]{1,0:T(8,128)(2,1)} %all-gather.14.cloned.1.call-done, bf16[2,4096,512]{2,1,0:T(8,128)(2,1)} %all-gather.16.cloned.1.call-done), kind=kOutput, calls=%fused_computation.38 | convolution fusion | flops 2147745792 | bytes 8912896 | tf_op jit(solution)/shard_map/dot_general | solution.py:56
  379.6 14.8 %psum.44 = f32[512]{0:T(512)S(1)} all-reduce(f32[512]{0:T(512)S(1)} %fusion.30), channel_id=1, replica_groups=mesh['sp'=4,'tp'=8] {'tp'}, use_global_device_ids=true, to_apply=%region_6.7 | all-reduce | flops 512 | bytes 4096 | tf_op jit(solution)/shard_map/psum | solution.py:60
  395.8 44.7 %all-gather.18.cloned.1.call-done = bf16[512,4096]{1,0:T(8,128)(2,1)} async-done(((bf16[512,512]{1,0:T(8,128)(2,1)}), bf16[512,4096]{1,0:T(8,128)(2,1)}) %all-gather.18.cloned.1.call-update) | async-done | bytes 4194320 | tf_op jit(solution)/shard_map/all_gather | solution.py:28
  440.5 3.2 fusion.3
  443.9 5.0 fusion.19
  449.0 2.4 fusion.22
  451.4 3.4 collective-permute-start.1
  456.5 5.0 fusion.100
  461.6 13.7 %all-reduce = (f32[512]{0:T(512)S(1)}, f32[512]{0:T(512)S(1)}) all-reduce(f32[512]{0:T(512)S(1)} %get-tuple-element.6, f32[512]{0:T(512)S(1)} %get-tuple-element.5), channel_id=1, replica_groups=mesh['sp'=4,'tp'=8] {'tp'}, use_global_device_ids=true, to_apply=%region_11.12 | all-reduce | flops 1024 | bytes 8192 | tf_op jit(solution)/shard_map/psum | solution.py:46
  476.6 45.9 %all-gather.20.cloned.1.call-done = bf16[512,4096]{1,0:T(8,128)(2,1)} async-done(((bf16[512,512]{1,0:T(8,128)(2,1)}), bf16[512,4096]{1,0:T(8,128)(2,1)}) %all-gather.20.cloned.1.call-update) | async-done | bytes 4194320 | tf_op jit(solution)/shard_map/all_gather | solution.py:55
  522.5 5.8 %fusion.25 = bf16[512,512]{1,0:T(8,128)(2,1)S(1)} fusion(bf16[512,4096]{1,0:T(8,128)(2,1)} %all-gather.20.cloned.1.call-done, bf16[2,4096,512]{2,1,0:T(8,128)(2,1)} %all-gather.16.cloned.1.call-done), kind=kOutput, calls=%fused_computation.39 | convolution fusion | flops 2147745792 | bytes 8912896 | tf_op jit(solution)/shard_map/dot_general | solution.py:56
  528.5 14.8 %psum.47 = f32[512]{0:T(512)S(1)} all-reduce(f32[512]{0:T(512)S(1)} %fusion.34), channel_id=1, replica_groups=mesh['sp'=4,'tp'=8] {'tp'}, use_global_device_ids=true, to_apply=%region_13.14 | all-reduce | flops 512 | bytes 4096 | tf_op jit(solution)/shard_map/psum | solution.py:60
  (63 shorter events, 10.4 us)
Async XLA Ops:
  6.5 2.8 copy-start.5
  6.5 2.9 copy-start.6
  6.5 2.9 copy-start.3
  6.5 3.0 copy-start.4
  6.5 52.0 %all-gather.8.cloned.1.call-start = ((), (), s32[]{:S(2)}) async-start(), calls=%async_computation | async-start | bytes 4718592 | tf_op jit(solution)/shard_map/all_gather | solution.py:28
  7.3 139.5 %all-gather.12.cloned.1.call-start = ((), (), s32[]{:S(2)}) async-start(), calls=%async_computation.2 | async-start | bytes 10485760 | tf_op jit(solution)/shard_map/all_gather | solution.py:23
  8.0 228.1 %all-gather.10.cloned.1.call-start = ((), (), s32[]{:S(2)}) async-start(), calls=%async_computation.1 | async-start | bytes 10485760 | tf_op jit(solution)/shard_map/all_gather | solution.py:22
  8.8 316.6 %all-gather.16.cloned.1.call-start = ((), (), s32[]{:S(2)}) async-start(), calls=%async_computation.4 | async-start | bytes 10485760 | tf_op jit(solution)/shard_map/all_gather | solution.py:24
  9.3 364.3 %all-gather.14.cloned.1.call-start = ((), (), s32[]{:S(2)}) async-start(), calls=%async_computation.3 | async-start | bytes 4718592 | tf_op jit(solution)/shard_map/all_gather | solution.py:55
  152.7 92.6 %copy-start.7 = (f32[2,512]{1,0:T(2,128)S(1)}, f32[2,512]{1,0:T(2,128)}, u32[]{:S(2)}) copy-start(f32[2,512]{1,0:T(2,128)} %param.16) | copy-start | bytes 12292
  242.0 5.0 collective-permute-start
  247.1 21.7 %copy-start.8 = (f32[2,512]{1,0:T(2,128)S(1)}, f32[2,512]{1,0:T(2,128)}, u32[]{:S(2)}) copy-start(f32[2,512]{1,0:T(2,128)} %param.19) | copy-start | bytes 12292
  268.7 171.8 %all-gather.18.cloned.1.call-start = ((), (), s32[]{:S(2)}) async-start(), calls=%async_computation.5 | async-start | bytes 4718592 | tf_op jit(solution)/shard_map/all_gather | solution.py:28
  268.8 125.7 %copy-start.2 = (bf16[512,512]{1,0:T(8,128)(2,1)S(1)}, bf16[512,512]{1,0:T(8,128)(2,1)}, u32[]{:S(2)}) copy-start(bf16[512,512]{1,0:T(8,128)(2,1)} %param.10) | copy-start | bytes 1572868
  395.5 127.0 %all-gather.20.cloned.1.call-start = ((), (), s32[]{:S(2)}) async-start(), calls=%async_computation.6 | async-start | bytes 4718592 | tf_op jit(solution)/shard_map/all_gather | solution.py:55
  440.5 3.4 copy-start.1
  440.5 8.5 %slice-start = ((s8[8388608]{0:T(1024)(128)(4,1)}), s8[4194304]{0:T(1024)(128)(4,1)S(1)}, s32[]{:S(2)}) async-start(s8[8388608]{0:T(1024)(128)(4,1)} %bitcast.194), calls=%async_computation.7 | async-start | bytes 8388608
  443.9 5.0 slice-start.1
  451.4 5.0 collective-permute-start.1
  476.6 66.7 %copy-start = (bf16[512,512]{1,0:T(8,128)(2,1)S(1)}, bf16[512,512]{1,0:T(8,128)(2,1)}, u32[]{:S(2)}) copy-start(bf16[512,512]{1,0:T(8,128)(2,1)} %fusion.33) | copy-start | bytes 1572868
Sparse Core Ops, SparseCore 0:
  9.0 49.5 all-gather.7
  60.4 86.2 all-gather.11
  148.6 87.4 all-gather.9
  237.8 87.4 all-gather.15
  326.8 46.8 all-gather.13
  395.7 44.7 all-gather.17
  476.7 45.7 all-gather.19
where the time goes:
time: 551 us
  waiting for transfers between devices  419 us (76%)
  blocking collectives  58.7 us (11%)
  matrix products  30.8 us (6%)
  other arithmetic  21.7 us (4%)
  between operations  13.8 us (3%)
  starting transfers between devices  7.2 us (1%)
    all_gather x2, waiting for transfers between devices, shards(): whole_mixed = lax.all_gather(mixed, 'tp', axis=1, tiled=True)  94.2 us
    all_gather x2, waiting for transfers between devices, shards(): gathered = lax.all_gather(stream, 'tp', axis=1, tiled=True)  93.7 us
    all_gather x1, waiting for transfers between devices, shards(): lax.all_gather(w_gate, 'sp', axis=1, tiled=True)  85.1 us
    all_gather x1, waiting for transfers between devices, shards(): lax.all_gather(w_value, 'sp', axis=1, tiled=True)  83.4 us
    all_gather x1, waiting for transfers between devices, shards(): lax.all_gather(w_out, 'sp', axis=1, tiled=True)  56.5 us
    psum x2, blocking collectives, shards(): total = lax.psum(jnp.sum(branch * branch, axis=-1), 'tp')  29.6 us
    psum x2, blocking collectives, shards(): lax.psum((jnp.sum(filtered, axis=-1), jnp.sum(filtered * filtered, axis=-...  29.1 us
    dot_general x2, matrix products, shards(): jnp.dot(whole_mixed, out_block, preferred_element_type=jnp.float32)  11.6 us
  transfers between devices with their start and end apart: 9, of which 9 were waited for; matrix products, arithmetic and copies ran while one was open for 4% of the time, Pallas kernels for 0%

commit v1 on v0

--- a/solution.py
+++ b/solution.py
@@ -25,7 +25,14 @@
     )
     stream = tokens
     for layer_index in range(layer_count):
-        gathered = lax.all_gather(stream, "tp", axis=1, tiled=True)
+        ring = [stream]
+        for hop in range(7):
+            ring.append(lax.ppermute(ring[-1], "tp", [(dev, (dev + 1) % 8) for dev in range(8)]))
+        gathered = jnp.roll(
+            jnp.concatenate(ring[::-1], axis=1),
+            (lax.axis_index("tp") + 1) * ring[0].shape[1],
+            axis=1,
+        )
         full_rows = gathered.astype(jnp.float32)
         scale_rows = lax.rsqrt(jnp.mean(full_rows * full_rows, axis=-1, keepdims=True) + 1e-06)
         normed = (full_rows * scale_rows * pre_gain[layer_index]).astype(jnp.bfloat16)

time: 551 us -> 529 us (0.960)
  waiting for transfers between devices: 419 us -> 394 us
    ppermute x0 -> x14, waiting for transfers between devices: none -> 146 us  [shards(): lax.ppermute(ring[-1], 'tp', [(dev, (dev + 1) % 8) for dev in range(8)])]
    all_gather x2 -> x0, waiting for transfers between devices: 93.7 us -> none  [shards(): gathered = lax.all_gather(stream, 'tp', axis=1, tiled=True)]
    all_gather x1, waiting for transfers between devices: 85.1 us -> 8.54 us  [shards(): lax.all_gather(w_gate, 'sp', axis=1, tiled=True)]
  transfers between devices with their start and end apart: 9 -> 21, of which waited for: 9 -> 21; matrix products, arithmetic and copies ran while one was open for 4% -> 5% of each run, Pallas kernels for 0% -> 0%
where the time goes in v1:
time: 529 us
  waiting for transfers between devices  394 us (74%)
  blocking collectives  58.5 us (11%)
  matrix products  28.4 us (5%)
  other arithmetic  23.4 us (4%)
  between operations  13.6 us (3%)
  starting transfers between devices  7.53 us (1%)
    ppermute x14, waiting for transfers between devices, shards(): lax.ppermute(ring[-1], 'tp', [(dev, (dev + 1) % 8) for dev in range(8)])  146 us
    all_gather x2, waiting for transfers between devices, shards(): whole_mixed = lax.all_gather(mixed, 'tp', axis=1, tiled=True)  94.4 us
    all_gather x1, waiting for transfers between devices, shards(): lax.all_gather(w_value, 'sp', axis=1, tiled=True)  83.3 us
    all_gather x1, waiting for transfers between devices, shards(): lax.all_gather(w_out, 'sp', axis=1, tiled=True)  56.4 us
    psum x2, blocking collectives, shards(): total = lax.psum(jnp.sum(branch * branch, axis=-1), 'tp')  29.6 us
    psum x2, blocking collectives, shards(): lax.psum((jnp.sum(filtered, axis=-1), jnp.sum(filtered * filtered, axis=-...  28.9 us
    dot_general x2, matrix products, shards(): jnp.dot(whole_mixed, out_block, preferred_element_type=jnp.float32)  11.6 us
  transfers between devices with their start and end apart: 21, of which 21 were waited for; matrix products, arithmetic and copies ran while one was open for 5% of the time, Pallas kernels for 0%

profile of v1, /device:TPU:0, one launch (start us, length us, event | category | flops | bytes accessed | tf_op | source)
XLA Modules:
  0.0 529.1 jit_solution(12006272173676621819)
XLA Ops:
  9.4 10.9 %collective-permute-done = bf16[512,512]{1,0:T(8,128)(2,1)S(1)} collective-permute-done((bf16[512,512]{1,0:T(8,128)(2,1)S(1)}, bf16[512,512]{1,0:T(8,128)(2,1)S(1)}, u32[]{:S(2)}, u32[]{:S(2)}) %collective-permute-start) | collective-permute-done | bytes 524320 | tf_op jit(solution)/shard_map/ppermute | solution.py:30
  20.3 10.4 %collective-permute-done.1 = bf16[512,512]{1,0:T(8,128)(2,1)S(1)} collective-permute-done((bf16[512,512]{1,0:T(8,128)(2,1)S(1)}, bf16[512,512]{1,0:T(8,128)(2,1)S(1)}, u32[]{:S(2)}, u32[]{:S(2)}) %collective-permute-start.1) | collective-permute-done | bytes 524320 | tf_op jit(solution)/shard_map/ppermute | solution.py:30
  30.7 10.4 %collective-permute-done.2 = bf16[512,512]{1,0:T(8,128)(2,1)S(1)} collective-permute-done((bf16[512,512]{1,0:T(8,128)(2,1)S(1)}, bf16[512,512]{1,0:T(8,128)(2,1)S(1)}, u32[]{:S(2)}, u32[]{:S(2)}) %collective-permute-start.2) | collective-permute-done | bytes 524320 | tf_op jit(solution)/shard_map/ppermute | solution.py:30
  41.1 10.4 %collective-permute-done.3 = bf16[512,512]{1,0:T(8,128)(2,1)S(1)} collective-permute-done((bf16[512,512]{1,0:T(8,128)(2,1)S(1)}, bf16[512,512]{1,0:T(8,128)(2,1)S(1)}, u32[]{:S(2)}, u32[]{:S(2)}) %collective-permute-start.3) | collective-permute-done | bytes 524320 | tf_op jit(solution)/shard_map/ppermute | solution.py:30
  51.5 10.4 %collective-permute-done.4 = bf16[512,512]{1,0:T(8,128)(2,1)S(1)} collective-permute-done((bf16[512,512]{1,0:T(8,128)(2,1)S(1)}, bf16[512,512]{1,0:T(8,128)(2,1)S(1)}, u32[]{:S(2)}, u32[]{:S(2)}) %collective-permute-start.4) | collective-permute-done | bytes 524320 | tf_op jit(solution)/shard_map/ppermute | solution.py:30
  62.0 10.4 %collective-permute-done.5 = bf16[512,512]{1,0:T(8,128)(2,1)} collective-permute-done((bf16[512,512]{1,0:T(8,128)(2,1)S(1)}, bf16[512,512]{1,0:T(8,128)(2,1)}, u32[]{:S(2)}, u32[]{:S(2)}) %collective-permute-start.5) | collective-permute-done | bytes 524320 | tf_op jit(solution)/shard_map/ppermute | solution.py:30
  72.5 10.6 %collective-permute-done.6 = bf16[512,512]{1,0:T(8,128)(2,1)} collective-permute-done((bf16[512,512]{1,0:T(8,128)(2,1)}, bf16[512,512]{1,0:T(8,128)(2,1)}, u32[]{:S(2)}, u32[]{:S(2)}) %collective-permute-start.6) | collective-permute-done | bytes 524320 | tf_op jit(solution)/shard_map/ppermute | solution.py:30
  90.9 8.5 %all-gather.8.cloned.1.call-done = bf16[2,4096,512]{2,1,0:T(8,128)(2,1)} async-done(((bf16[2,1024,512]{2,1,0:T(8,128)(2,1)}), bf16[2,4096,512]{2,1,0:T(8,128)(2,1)}) %all-gather.8.cloned.1.call-update) | async-done | bytes 8388624 | tf_op jit(solution)/shard_map/all_gather | solution.py:23
  99.4 6.0 %fusion.23 = f32[512,512]{1,0:T(8,128)S(1)} fusion(bf16[2,4096,512]{2,1,0:T(8,128)(2,1)} %all-gather.8.cloned.1.call-done, bf16[512,4096]{1,0:T(8,128)(2,1)} %get-tuple-element.19, f32[4096]{0:T(1024)S(1)} %bitcast.122, f32[512]{0:T(512)S(1)} %add_rsqrt_fusion.5), kind=kOutput, calls=%fused_computation.41 | convolution fusion | flops 2156658688 | bytes 9455616 | tf_op jit(solution)/shard_map/dot_general | solution.py:43
  105.5 83.3 %all-gather.6.cloned.1.call-done = bf16[2,4096,512]{2,1,0:T(8,128)(2,1)} async-done(((bf16[2,1024,512]{2,1,0:T(8,128)(2,1)}), bf16[2,4096,512]{2,1,0:T(8,128)(2,1)}) %all-gather.6.cloned.1.call-update) | async-done | bytes 8388624 | tf_op jit(solution)/shard_map/all_gather | solution.py:22
  204.8 15.3 %all-reduce.1 = (f32[512]{0:T(512)S(1)}, f32[512]{0:T(512)S(1)}) all-reduce(f32[512]{0:T(512)S(1)} %get-tuple-element.9, f32[512]{0:T(512)S(1)} %get-tuple-element.8), channel_id=1, replica_groups=mesh['sp'=4,'tp'=8] {'tp'}, use_global_device_ids=true, to_apply=%region_4.6 | all-reduce | flops 1024 | bytes 8192 | tf_op jit(solution)/shard_map/psum | solution.py:53
  221.7 56.4 %all-gather.12.cloned.1.call-done = bf16[2,4096,512]{2,1,0:T(8,128)(2,1)} async-done(((bf16[2,1024,512]{2,1,0:T(8,128)(2,1)}), bf16[2,4096,512]{2,1,0:T(8,128)(2,1)}) %all-gather.12.cloned.1.call-update) | async-done | bytes 8388624 | tf_op jit(solution)/shard_map/all_gather | solution.py:24
  278.2 48.4 %all-gather.10.cloned.1.call-done = bf16[512,4096]{1,0:T(8,128)(2,1)} async-done(((bf16[512,512]{1,0:T(8,128)(2,1)}), bf16[512,4096]{1,0:T(8,128)(2,1)}) %all-gather.10.cloned.1.call-update) | async-done | bytes 4194320 | tf_op jit(solution)/shard_map/all_gather | solution.py:62
  332.5 14.8 %psum.44 = f32[512]{0:T(512)S(1)} all-reduce(f32[512]{0:T(512)S(1)} %fusion.32), channel_id=1, replica_groups=mesh['sp'=4,'tp'=8] {'tp'}, use_global_device_ids=true, to_apply=%region_6.8 | all-reduce | flops 512 | bytes 4096 | tf_op jit(solution)/shard_map/psum | solution.py:67
  347.6 10.4 %collective-permute-done.8 = bf16[512,512]{1,0:T(8,128)(2,1)S(1)} collective-permute-done((bf16[512,512]{1,0:T(8,128)(2,1)S(1)}, bf16[512,512]{1,0:T(8,128)(2,1)S(1)}, u32[]{:S(2)}, u32[]{:S(2)}) %collective-permute-start.8) | collective-permute-done | bytes 524320 | tf_op jit(solution)/shard_map/ppermute | solution.py:30
  358.0 10.4 %collective-permute-done.9 = bf16[512,512]{1,0:T(8,128)(2,1)S(1)} collective-permute-done((bf16[512,512]{1,0:T(8,128)(2,1)S(1)}, bf16[512,512]{1,0:T(8,128)(2,1)S(1)}, u32[]{:S(2)}, u32[]{:S(2)}) %collective-permute-start.9) | collective-permute-done | bytes 524320 | tf_op jit(solution)/shard_map/ppermute | solution.py:30
  368.4 10.4 %collective-permute-done.10 = bf16[512,512]{1,0:T(8,128)(2,1)S(1)} collective-permute-done((bf16[512,512]{1,0:T(8,128)(2,1)S(1)}, bf16[512,512]{1,0:T(8,128)(2,1)S(1)}, u32[]{:S(2)}, u32[]{:S(2)}) %collective-permute-start.10) | collective-permute-done | bytes 524320 | tf_op jit(solution)/shard_map/ppermute | solution.py:30
  378.9 10.4 %collective-permute-done.11 = bf16[512,512]{1,0:T(8,128)(2,1)S(1)} collective-permute-done((bf16[512,512]{1,0:T(8,128)(2,1)S(1)}, bf16[512,512]{1,0:T(8,128)(2,1)S(1)}, u32[]{:S(2)}, u32[]{:S(2)}) %collective-permute-start.11) | collective-permute-done | bytes 524320 | tf_op jit(solution)/shard_map/ppermute | solution.py:30
  389.3 10.4 %collective-permute-done.12 = bf16[512,512]{1,0:T(8,128)(2,1)S(1)} collective-permute-done((bf16[512,512]{1,0:T(8,128)(2,1)S(1)}, bf16[512,512]{1,0:T(8,128)(2,1)S(1)}, u32[]{:S(2)}, u32[]{:S(2)}) %collective-permute-start.12) | collective-permute-done | bytes 524320 | tf_op jit(solution)/shard_map/ppermute | solution.py:30
  399.7 10.4 %collective-permute-done.13 = bf16[512,512]{1,0:T(8,128)(2,1)S(1)} collective-permute-done((bf16[512,512]{1,0:T(8,128)(2,1)S(1)}, bf16[512,512]{1,0:T(8,128)(2,1)S(1)}, u32[]{:S(2)}, u32[]{:S(2)}) %collective-permute-start.13) | collective-permute-done | bytes 524320 | tf_op jit(solution)/shard_map/ppermute | solution.py:30
  410.1 10.4 %collective-permute-done.14 = bf16[512,512]{1,0:T(8,128)(2,1)S(1)} collective-permute-done((bf16[512,512]{1,0:T(8,128)(2,1)S(1)}, bf16[512,512]{1,0:T(8,128)(2,1)S(1)}, u32[]{:S(2)}, u32[]{:S(2)}) %collective-permute-start.14) | collective-permute-done | bytes 524320 | tf_op jit(solution)/shard_map/ppermute | solution.py:30
  439.8 13.6 %all-reduce = (f32[512]{0:T(512)S(1)}, f32[512]{0:T(512)S(1)}) all-reduce(f32[512]{0:T(512)S(1)} %get-tuple-element.7, f32[512]{0:T(512)S(1)} %get-tuple-element.6), channel_id=1, replica_groups=mesh['sp'=4,'tp'=8] {'tp'}, use_global_device_ids=true, to_apply=%region_11.13 | all-reduce | flops 1024 | bytes 8192 | tf_op jit(solution)/shard_map/psum | solution.py:53
  454.7 46.0 %all-gather.14.cloned.1.call-done = bf16[512,4096]{1,0:T(8,128)(2,1)} async-done(((bf16[512,512]{1,0:T(8,128)(2,1)}), bf16[512,4096]{1,0:T(8,128)(2,1)}) %all-gather.14.cloned.1.call-update) | async-done | bytes 4194320 | tf_op jit(solution)/shard_map/all_gather | solution.py:62
  506.7 14.8 %psum.47 = f32[512]{0:T(512)S(1)} all-reduce(f32[512]{0:T(512)S(1)} %fusion.36), channel_id=1, replica_groups=mesh['sp'=4,'tp'=8] {'tp'}, use_global_device_ids=true, to_apply=%region_13.15 | all-reduce | flops 512 | bytes 4096 | tf_op jit(solution)/shard_map/psum | solution.py:67
  (102 shorter events, 61.9 us)
Async XLA Ops:
  6.5 55.4 %copy-start.1 = (f32[2,31,512]{2,0,1:T(2,128)S(1)}, f32[2,31,512]{2,0,1:T(2,128)}, u32[]{:S(2)}) copy-start(f32[2,31,512]{2,0,1:T(2,128)} %param.16) | copy-start | bytes 380932
  6.5 65.8 %copy-start.4 = (f32[2,512]{1,0:T(2,128)S(1)}, f32[2,512]{1,0:T(2,128)}, u32[]{:S(2)}) copy-start(f32[2,512]{1,0:T(2,128)} %param.19) | copy-start | bytes 12292
  6.5 92.9 %all-gather.8.cloned.1.call-start = ((), (), s32[]{:S(2)}) async-start(), calls=%async_computation.1 | async-start | bytes 10485760 | tf_op jit(solution)/shard_map/all_gather | solution.py:23
  7.3 181.5 %all-gather.6.cloned.1.call-start = ((), (), s32[]{:S(2)}) async-start(), calls=%async_computation | async-start | bytes 10485760 | tf_op jit(solution)/shard_map/all_gather | solution.py:22
  8.0 270.1 %all-gather.12.cloned.1.call-start = ((), (), s32[]{:S(2)}) async-start(), calls=%async_computation.3 | async-start | bytes 10485760 | tf_op jit(solution)/shard_map/all_gather | solution.py:24
  8.8 317.7 %all-gather.10.cloned.1.call-start = ((), (), s32[]{:S(2)}) async-start(), calls=%async_computation.2 | async-start | bytes 4718592 | tf_op jit(solution)/shard_map/all_gather | solution.py:62
  8.8 11.4 %collective-permute-start = (bf16[512,512]{1,0:T(8,128)(2,1)S(1)}, bf16[512,512]{1,0:T(8,128)(2,1)S(1)}, u32[]{:S(2)}, u32[]{:S(2)}) collective-permute-start(bf16[512,512]{1,0:T(8,128)(2,1)S(1)} %copy-done), channel_id=1, source_target_pairs={{0,1},{1,2},{2,3},{3,4},{4,5},{5,6},{6,7},{7,0},{8,9},{9,10},{10,1... | collective-permute-start | bytes 1572872 | tf_op jit(solution)/shard_map/ppermute | solution.py:30
  20.3 10.4 %collective-permute-start.1 = (bf16[512,512]{1,0:T(8,128)(2,1)S(1)}, bf16[512,512]{1,0:T(8,128)(2,1)S(1)}, u32[]{:S(2)}, u32[]{:S(2)}) collective-permute-start(bf16[512,512]{1,0:T(8,128)(2,1)S(1)} %collective-permute-done), channel_id=1, source_target_pairs={{0,1},{1,2},{2,3},{3,4},{4,5},{5,6},{6,7},{7,0},{8,9},{9,10},{10,1... | collective-permute-start | bytes 1572872 | tf_op jit(solution)/shard_map/ppermute | solution.py:30
  30.7 10.4 %collective-permute-start.2 = (bf16[512,512]{1,0:T(8,128)(2,1)S(1)}, bf16[512,512]{1,0:T(8,128)(2,1)S(1)}, u32[]{:S(2)}, u32[]{:S(2)}) collective-permute-start(bf16[512,512]{1,0:T(8,128)(2,1)S(1)} %collective-permute-done.1), channel_id=1, source_target_pairs={{0,1},{1,2},{2,3},{3,4},{4,5},{5,6},{6,7},{7,0},{8,9},{9,10},{10,1... | collective-permute-start | bytes 1572872 | tf_op jit(solution)/shard_map/ppermute | solution.py:30
  41.1 10.4 %collective-permute-start.3 = (bf16[512,512]{1,0:T(8,128)(2,1)S(1)}, bf16[512,512]{1,0:T(8,128)(2,1)S(1)}, u32[]{:S(2)}, u32[]{:S(2)}) collective-permute-start(bf16[512,512]{1,0:T(8,128)(2,1)S(1)} %collective-permute-done.2), channel_id=1, source_target_pairs={{0,1},{1,2},{2,3},{3,4},{4,5},{5,6},{6,7},{7,0},{8,9},{9,10},{10,1... | collective-permute-start | bytes 1572872 | tf_op jit(solution)/shard_map/ppermute | solution.py:30
  51.5 10.4 %collective-permute-start.4 = (bf16[512,512]{1,0:T(8,128)(2,1)S(1)}, bf16[512,512]{1,0:T(8,128)(2,1)S(1)}, u32[]{:S(2)}, u32[]{:S(2)}) collective-permute-start(bf16[512,512]{1,0:T(8,128)(2,1)S(1)} %collective-permute-done.3), channel_id=1, source_target_pairs={{0,1},{1,2},{2,3},{3,4},{4,5},{5,6},{6,7},{7,0},{8,9},{9,10},{10,1... | collective-permute-start | bytes 1572872 | tf_op jit(solution)/shard_map/ppermute | solution.py:30
  61.9 10.5 %collective-permute-start.5 = (bf16[512,512]{1,0:T(8,128)(2,1)S(1)}, bf16[512,512]{1,0:T(8,128)(2,1)}, u32[]{:S(2)}, u32[]{:S(2)}) collective-permute-start(bf16[512,512]{1,0:T(8,128)(2,1)S(1)} %collective-permute-done.4), channel_id=1, source_target_pairs={{0,1},{1,2},{2,3},{3,4},{4,5},{5,6},{6,7},{7,0},{8,9},{9,10},{10,1... | collective-permute-start | bytes 1572872 | tf_op jit(solution)/shard_map/ppermute | solution.py:30
  72.4 10.7 %collective-permute-start.6 = (bf16[512,512]{1,0:T(8,128)(2,1)}, bf16[512,512]{1,0:T(8,128)(2,1)}, u32[]{:S(2)}, u32[]{:S(2)}) collective-permute-start(bf16[512,512]{1,0:T(8,128)(2,1)} %collective-permute-done.5), channel_id=1, source_target_pairs={{0,1},{1,2},{2,3},{3,4},{4,5},{5,6},{6,7},{7,0},{8,9},{9,10},{10,1... | collective-permute-start | bytes 1572872 | tf_op jit(solution)/shard_map/ppermute | solution.py:30
  105.4 92.6 %copy-start.5 = (f32[2,512]{1,0:T(2,128)S(1)}, f32[2,512]{1,0:T(2,128)}, u32[]{:S(2)}) copy-start(f32[2,512]{1,0:T(2,128)} %param.18) | copy-start | bytes 12292
  194.7 5.0 collective-permute-start.7
  221.5 279.3 %all-gather.14.cloned.1.call-start = ((), (), s32[]{:S(2)}) async-start(), calls=%async_computation.4 | async-start | bytes 4718592 | tf_op jit(solution)/shard_map/all_gather | solution.py:62
  347.6 10.5 %collective-permute-start.8 = (bf16[512,512]{1,0:T(8,128)(2,1)S(1)}, bf16[512,512]{1,0:T(8,128)(2,1)S(1)}, u32[]{:S(2)}, u32[]{:S(2)}) collective-permute-start(bf16[512,512]{1,0:T(8,128)(2,1)S(1)} %fusion.35), channel_id=1, source_target_pairs={{0,1},{1,2},{2,3},{3,4},{4,5},{5,6},{6,7},{7,0},{8,9},{9,10},{10,1... | collective-permute-start | bytes 1572872 | tf_op jit(solution)/shard_map/ppermute | solution.py:30
  358.0 10.4 %collective-permute-start.9 = (bf16[512,512]{1,0:T(8,128)(2,1)S(1)}, bf16[512,512]{1,0:T(8,128)(2,1)S(1)}, u32[]{:S(2)}, u32[]{:S(2)}) collective-permute-start(bf16[512,512]{1,0:T(8,128)(2,1)S(1)} %collective-permute-done.8), channel_id=1, source_target_pairs={{0,1},{1,2},{2,3},{3,4},{4,5},{5,6},{6,7},{7,0},{8,9},{9,10},{10,1... | collective-permute-start | bytes 1572872 | tf_op jit(solution)/shard_map/ppermute | solution.py:30
  368.4 10.4 %collective-permute-start.10 = (bf16[512,512]{1,0:T(8,128)(2,1)S(1)}, bf16[512,512]{1,0:T(8,128)(2,1)S(1)}, u32[]{:S(2)}, u32[]{:S(2)}) collective-permute-start(bf16[512,512]{1,0:T(8,128)(2,1)S(1)} %collective-permute-done.9), channel_id=1, source_target_pairs={{0,1},{1,2},{2,3},{3,4},{4,5},{5,6},{6,7},{7,0},{8,9},{9,10},{10,1... | collective-permute-start | bytes 1572872 | tf_op jit(solution)/shard_map/ppermute | solution.py:30
  378.8 10.4 %collective-permute-start.11 = (bf16[512,512]{1,0:T(8,128)(2,1)S(1)}, bf16[512,512]{1,0:T(8,128)(2,1)S(1)}, u32[]{:S(2)}, u32[]{:S(2)}) collective-permute-start(bf16[512,512]{1,0:T(8,128)(2,1)S(1)} %collective-permute-done.10), channel_id=1, source_target_pairs={{0,1},{1,2},{2,3},{3,4},{4,5},{5,6},{6,7},{7,0},{8,9},{9,10},{10,1... | collective-permute-start | bytes 1572872 | tf_op jit(solution)/shard_map/ppermute | solution.py:30
  389.3 10.4 %collective-permute-start.12 = (bf16[512,512]{1,0:T(8,128)(2,1)S(1)}, bf16[512,512]{1,0:T(8,128)(2,1)S(1)}, u32[]{:S(2)}, u32[]{:S(2)}) collective-permute-start(bf16[512,512]{1,0:T(8,128)(2,1)S(1)} %collective-permute-done.11), channel_id=1, source_target_pairs={{0,1},{1,2},{2,3},{3,4},{4,5},{5,6},{6,7},{7,0},{8,9},{9,10},{10,1... | collective-permute-start | bytes 1572872 | tf_op jit(solution)/shard_map/ppermute | solution.py:30
  399.7 10.4 %collective-permute-start.13 = (bf16[512,512]{1,0:T(8,128)(2,1)S(1)}, bf16[512,512]{1,0:T(8,128)(2,1)S(1)}, u32[]{:S(2)}, u32[]{:S(2)}) collective-permute-start(bf16[512,512]{1,0:T(8,128)(2,1)S(1)} %collective-permute-done.12), channel_id=1, source_target_pairs={{0,1},{1,2},{2,3},{3,4},{4,5},{5,6},{6,7},{7,0},{8,9},{9,10},{10,1... | collective-permute-start | bytes 1572872 | tf_op jit(solution)/shard_map/ppermute | solution.py:30
  410.1 10.4 %collective-permute-start.14 = (bf16[512,512]{1,0:T(8,128)(2,1)S(1)}, bf16[512,512]{1,0:T(8,128)(2,1)S(1)}, u32[]{:S(2)}, u32[]{:S(2)}) collective-permute-start(bf16[512,512]{1,0:T(8,128)(2,1)S(1)} %collective-permute-done.13), channel_id=1, source_target_pairs={{0,1},{1,2},{2,3},{3,4},{4,5},{5,6},{6,7},{7,0},{8,9},{9,10},{10,1... | collective-permute-start | bytes 1572872 | tf_op jit(solution)/shard_map/ppermute | solution.py:30
  429.9 4.7 collective-permute-start.15
  (8 other events, 152.1 us)
Sparse Core Ops, SparseCore 0:
  9.2 90.1 all-gather.7
  101.3 87.4 all-gather.5
  190.6 87.4 all-gather.11
  279.6 46.8 all-gather.9
  454.8 45.8 all-gather.13
